TPU v7x, 32 devices: a whole 2x2x4 slice. The times are simulated.
32 devices in a mesh: grp: 2 (over y), fs: 4 (over z), tp: 4 (over x, core).
Axes of the slice: x: 2, y: 2, z: 4, core: 2. Of those that a mesh axis runs over, the one named last changes fastest.
Arguments:
- tokens: bfloat16 [1792, 2048], P(('grp', 'fs'), 'tp'), parts along dimension 0, may hold values from -6 to 6
- route_ids: int32 [1792, 2], P(('grp', 'fs')), parts along dimension 0, may hold values from 0 to 3, all different within a row; in each aligned block of 224 rows (0 to 223, 224 to 447, ...) at most 168 rows name the same one
- route_weights: float32 [1792, 2], P(('grp', 'fs')), parts along dimension 0, may hold values from 0.25 to 1
- norm_gain: float32 [2048], P('fs'), may hold values from 0.1 to 1.9
- gate_master: float32 [4, 2048, 512], P(None, 'fs', 'tp'), may hold values from -0.125 to 0.125
- up_master: float32 [4, 2048, 512], P(None, 'fs', 'tp'), may hold values from -0.125 to 0.125
- down_master: float32 [4, 2048, 512], P(None, 'fs', 'tp'), may hold values from -0.25 to 0.25
Outputs:
- gate_serve: bfloat16 [8, 2048, 512], P(('grp', 'fs'), None, 'tp'), parts along dimension 0
- up_serve: bfloat16 [8, 2048, 512], P(('grp', 'fs'), None, 'tp'), parts along dimension 0
- down_serve: bfloat16 [8, 2048, 512], P(('grp', 'fs'), None, 'tp'), parts along dimension 0
- moe_output: bfloat16 [1792, 2048], P(('grp', 'fs'), 'tp'), parts along dimension 0
There are 2 independent parts, one for each index of `grp`. A program takes and returns all parts, laid end to end along the dimension named above; an argument that names none is the same for every part. Nothing has to cross between parts.
Inputs may be any that keep to these rules, and one draw needn't show every extreme that they name: `route_ids`: the 2 experts of a row differ; within the rows of one index of fs (aligned blocks of 224 rows) no expert is named more than 168 times.
All inputs are finite; a program needn't handle non-finite values.
Results may differ from a plain program's by a relative error of at most 0.012.
Values may be sent and summed in bfloat16 or wider, within the bound.
A program may use at most 64 MiB of HBM per device.

v0:
```python
import jax
import jax.numpy as jnp
from jax import lax
from jax.sharding import PartitionSpec as P

norm_epsilon = 1e-06


def slot_numbers(route_ids, experts, capacity):
    flat_ids = route_ids.reshape(-1)
    onehot = (flat_ids[:, None] == jnp.arange(experts, dtype=jnp.int32)[None, :]).astype(jnp.int32)
    before = jnp.cumsum(onehot, axis=0) - onehot
    position = jnp.sum(before * onehot, axis=1)
    return (flat_ids * capacity + position).reshape(route_ids.shape)


def local(tokens, route_ids, route_weights, norm_gain, gate_master, up_master, down_master):
    experts = gate_master.shape[0]
    shards = lax.axis_size("fs")
    columns = lax.axis_size("tp")
    per_device = experts // shards
    tok_rows = route_ids.shape[0]
    top_count = route_ids.shape[1]
    local_width = tokens.shape[1]
    model_width = local_width * columns
    capacity = max(2, 3 * tok_rows * top_count // (2 * experts))
    row_gain = norm_gain[None, :, None]
    gate_half = (gate_master * row_gain).astype(jnp.bfloat16)
    up_half = (up_master * row_gain).astype(jnp.bfloat16)
    down_half = down_master.astype(jnp.bfloat16)
    gate_serve, up_serve, down_serve = (
        lax.all_to_all(gate_half, "fs", split_axis=0, concat_axis=1, tiled=True),
        lax.all_to_all(up_half, "fs", split_axis=0, concat_axis=1, tiled=True),
        lax.all_to_all(down_half, "fs", split_axis=0, concat_axis=1, tiled=True),
    )
    slot_ids = slot_numbers(route_ids, experts, capacity)
    slot_range = jnp.arange(experts * capacity, dtype=jnp.int32)
    selects = [
        (slot_ids[:, rank_slot, None] == slot_range[None, :]).astype(jnp.bfloat16)
        for rank_slot in range(top_count)
    ]
    placing = selects[0]
    for extra in selects[1:]:
        placing = placing + extra
    local_values = tokens.astype(jnp.float32)
    squares = lax.psum(jnp.sum(local_values * local_values, axis=1), "tp")
    inverse = lax.rsqrt(squares / model_width + norm_epsilon)[:, None]
    normed = (local_values * inverse).astype(jnp.bfloat16)
    buffer = jnp.einsum("ts,td->sd", placing, normed, preferred_element_type=jnp.float32).astype(
        jnp.bfloat16
    )
    arrived = lax.all_to_all(
        buffer.reshape(shards, per_device * capacity, local_width),
        "fs",
        split_axis=0,
        concat_axis=0,
        tiled=True,
    )
    arrived = arrived.reshape(shards, per_device, capacity, local_width)
    partial_value = lax.all_gather(arrived, "tp", axis=3, tiled=True)
    gate_sum = jnp.einsum(
        "sxcd,xdf->xscf", partial_value, gate_serve, preferred_element_type=jnp.float32
    )
    up_sum = jnp.einsum(
        "sxcd,xdf->xscf", partial_value, up_serve, preferred_element_type=jnp.float32
    )
    hidden = (jax.nn.silu(gate_sum) * up_sum).astype(jnp.bfloat16)
    products = jnp.einsum("xdf,xscf->dsxc", down_serve, hidden, preferred_element_type=jnp.float32)
    summed = lax.psum_scatter(
        products.reshape(local_width * lax.axis_size("tp"), shards * per_device * capacity).astype(
            jnp.bfloat16
        ),
        "tp",
        scatter_dimension=0,
        tiled=True,
    )
    returned = lax.all_to_all(
        summed.reshape(local_width, shards, per_device * capacity),
        "fs",
        split_axis=1,
        concat_axis=1,
        tiled=True,
    )
    returned = returned.reshape(local_width, experts * capacity)
    combined = jnp.zeros((tok_rows, local_width), jnp.float32)
    for rank_slot in range(top_count):
        picked = jnp.einsum(
            "ts,ds->td", selects[rank_slot], returned, preferred_element_type=jnp.float32
        )
        combined = combined + route_weights[:, rank_slot : rank_slot + 1] * picked
    return (gate_serve, up_serve, down_serve, combined.astype(jnp.bfloat16))


def solution(mesh):
    placed = (
        P(("grp", "fs"), "tp"),
        P(("grp", "fs"), None),
        P(("grp", "fs"), None),
        P("fs"),
        P(None, "fs", "tp"),
        P(None, "fs", "tp"),
        P(None, "fs", "tp"),
    )
    return jax.shard_map(
        local,
        mesh=mesh,
        in_specs=placed,
        out_specs=(
            P(("grp", "fs"), None, "tp"),
            P(("grp", "fs"), None, "tp"),
            P(("grp", "fs"), None, "tp"),
            P(("grp", "fs"), "tp"),
        ),
        check_vma=False,
    )
```

profile of v0, /device:TPU:0, one launch (start us, length us, event | category | flops | bytes accessed | tf_op | source)
XLA Modules:
  0.0 170.7 jit_solution(8881094231520576288)
XLA Ops:
  7.2 0.0 copy-start.7
  7.2 0.0 copy-start.5
  7.2 0.0 copy-start.4
  7.2 0.0 all-gather.3.cloned.1.call-start
  7.2 0.9 copy.17
  8.2 0.1 eq.52
  8.4 1.2 reduce-window.6
  9.6 0.2 slice_reduce_fusion
  9.8 0.2 reduce-window.9
  10.0 0.1 add_bitcast_fusion
  10.1 0.1 reduce_sum.21
  10.3 0.1 copy.18
  10.3 0.7 multiply_add_fusion
  11.0 1.1 fusion.5
  12.1 8.4 %psum.7 = f32[224]{0:T(256)S(1)} all-reduce(f32[224]{0:T(256)S(1)} %fusion.5), channel_id=1, replica_groups=mesh['grp'=2,'fs'=4,'tp'=4] {'tp'}, use_global_device_ids=true, to_apply=%region_4.5 | all-reduce | flops 224 | bytes 1792 | tf_op jit(solution)/shard_map/psum | solution.py:46
  20.5 1.5 convolution_convert_fusion.1
  22.0 21.6 %all_to_all.46 = bf16[4,168,512]{2,1,0:T(8,128)(2,1)} all-to-all(bf16[4,168,512]{2,1,0:T(8,128)(2,1)S(1)} %bitcast.48), channel_id=1, replica_groups=mesh['grp'=2,'fs'=4,'tp'=4] {'fs'}, dimensions={0} | all-to-all | bytes 1376256 | tf_op jit(solution)/shard_map/all_to_all | solution.py:52
  43.5 0.0 all-gather.3.cloned.1.call-update
  43.6 0.0 copy-done.7
  43.6 0.0 copy-done.5
  43.6 0.0 copy-done.4
  43.6 0.0 copy-start.3
  43.6 1.0 multiply_convert_fusion
  44.6 16.2 %all_to_all.47 = bf16[4,512,128]{2,1,0:T(8,128)(2,1)S(1)} all-to-all(bf16[4,512,128]{2,1,0:T(8,128)(2,1)S(1)} %get-tuple-element.9), channel_id=1, replica_groups=mesh['grp'=2,'fs'=4,'tp'=4] {'fs'}, dimensions={0} | all-to-all | bytes 1048576 | tf_op jit(solution)/shard_map/all_to_all | solution.py:32
  60.9 3.5 %all-to-all-start.1 = ((bf16[4,512,128]{2,1,0:T(8,128)(2,1)}), bf16[4,512,128]{2,1,0:T(8,128)(2,1)S(1)}, u32[]{:S(2)}, u32[]{:S(2)}) async-start(bf16[4,512,128]{2,1,0:T(8,128)(2,1)} %get-tuple-element.8), calls=%async_computation.1 | async-start | bytes 1048576 | tf_op jit(solution)/shard_map/all_to_all | solution.py:33
  64.4 0.0 copy-done.3
  64.4 0.9 convert_element_type.49
  65.2 12.6 %all-to-all-done.1 = bf16[4,512,128]{2,1,0:T(8,128)(2,1)S(1)} async-done(((bf16[4,512,128]{2,1,0:T(8,128)(2,1)}), bf16[4,512,128]{2,1,0:T(8,128)(2,1)S(1)}, u32[]{:S(2)}, u32[]{:S(2)}) %all-to-all-start.1) | async-done | bytes 524320 | tf_op jit(solution)/shard_map/all_to_all | solution.py:33
  77.9 0.0 copy-start.1
  77.9 4.1 %all-to-all-start.2 = ((bf16[4,512,128]{2,1,0:T(8,128)(2,1)}), bf16[4,512,128]{2,1,0:T(8,128)(2,1)}, u32[]{:S(2)}, u32[]{:S(2)}) async-start(bf16[4,512,128]{2,1,0:T(8,128)(2,1)} %convert_element_type.49), calls=%async_computation.2 | async-start | bytes 1048576 | tf_op jit(solution)/shard_map/all_to_all | solution.py:34
  82.0 0.0 reduce-scatter.2.cloned.1.call-start
  82.1 0.0 copy-done.1
  82.1 0.0 all-gather.3.cloned.1.call-done
  82.1 0.0 copy-start
  82.1 3.5 %fusion.27 = f32[4,168,128]{2,1,0:T(8,128)} fusion(bf16[4,168,2048]{2,1,0:T(8,128)(2,1)} %all-gather.3.cloned.1.call-done, bf16[2048,128,1]{1,0,2:T(8,128)(2,1)S(1)} %bitcast.41), kind=kOutput, calls=%fused_computation.44 | convolution fusion | flops 352321536 | bytes 3620864 | tf_op jit(solution)/shard_map/sxcd,xdf->xscf/dot_general | solution.py:61
  85.7 10.5 %all-to-all-done.2 = bf16[4,512,128]{2,1,0:T(8,128)(2,1)} async-done(((bf16[4,512,128]{2,1,0:T(8,128)(2,1)}), bf16[4,512,128]{2,1,0:T(8,128)(2,1)}, u32[]{:S(2)}, u32[]{:S(2)}) %all-to-all-start.2) | async-done | bytes 524320 | tf_op jit(solution)/shard_map/all_to_all | solution.py:34
  96.1 0.0 copy-done
  96.1 5.8 %convolution_convert_fusion = bf16[4,168,2048]{2,1,0:T(8,128)(2,1)} fusion(bf16[2048,128,1]{1,0,2:T(8,128)(2,1)} %bitcast.13, bf16[4,168,2048]{2,1,0:T(8,128)(2,1)S(1)} %copy-done, bf16[2048,128,1]{1,0,2:T(8,128)(2,1)} %bitcast.43, f32[4,168,128]{2,1,0:T(8,128)} %fusion.27), kind=kOutput, calls=%fused_computation | convolution fusion | flops 706535424 | bytes 6897664 | tf_op jit(solution)/shard_map/xdf,xscf->dsxc/dot_general | solution.py:68
  102.0 0.0 copy-start.6
  102.0 0.0 reduce-scatter.2.cloned.1.call-update
  102.0 0.0 copy-start.2
  102.0 34.5 %reduce-scatter.2.cloned.1.call-done = bf16[512,672]{0,1:T(8,128)(2,1)} async-done(((bf16[2048,672]{0,1:T(8,128)(2,1)}), bf16[512,672]{0,1:T(8,128)(2,1)}) %reduce-scatter.2.cloned.1.call-update) | async-done | bytes 688144 | tf_op jit(solution)/shard_map/reduce_scatter | solution.py:69
  136.5 4.6 %all-to-all-start.4 = ((bf16[512,4,168]{0,2,1:T(8,128)(2,1)}), bf16[512,4,168]{0,2,1:T(8,128)(2,1)S(1)}, u32[]{:S(2)}, u32[]{:S(2)}) async-start(bf16[512,4,168]{0,2,1:T(8,128)(2,1)} %bitcast.47), calls=%async_computation.5 | async-start | bytes 1376256 | tf_op jit(solution)/shard_map/all_to_all | solution.py:77
  141.1 0.0 copy-done.6
  141.1 17.8 %all-to-all-done.4 = bf16[512,4,168]{0,2,1:T(8,128)(2,1)S(1)} async-done(((bf16[512,4,168]{0,2,1:T(8,128)(2,1)}), bf16[512,4,168]{0,2,1:T(8,128)(2,1)S(1)}, u32[]{:S(2)}, u32[]{:S(2)}) %all-to-all-start.4) | async-done | bytes 688160 | tf_op jit(solution)/shard_map/all_to_all | solution.py:77
  158.9 0.4 convolution_multiply_fusion.1
  159.3 1.1 fusion.1
  160.4 0.8 copy.25
  161.2 0.0 copy-done.2
  161.2 0.8 copy.26
  162.0 1.9 %copy.27 = bf16[1,2048,128]{2,1,0:T(8,128)(2,1)} copy(bf16[1,2048,128]{2,1,0:T(8,128)(2,1)} %bitcast.2) | data formatting | bytes 1048576
  (8 shorter events, 0.1 us)
Async XLA Ops:
  7.2 36.4 %copy-start.7 = (f32[512]{0:T(512)S(1)}, f32[512]{0:T(512)}, u32[]{:S(2)}) copy-start(f32[512]{0:T(512)} %param.10) | copy-start | bytes 6148
  7.2 36.4 %copy-start.5 = (f32[4,512,128]{2,1,0:T(8,128)S(1)}, f32[4,512,128]{2,1,0:T(8,128)}, u32[]{:S(2)}) copy-start(f32[4,512,128]{2,1,0:T(8,128)} %param.11) | copy-start | bytes 3145732
  7.2 36.4 %copy-start.4 = (f32[4,512,128]{2,1,0:T(8,128)S(1)}, f32[4,512,128]{2,1,0:T(8,128)}, u32[]{:S(2)}) copy-start(f32[4,512,128]{2,1,0:T(8,128)} %param.12) | copy-start | bytes 3145732
  7.2 74.9 %all-gather.3.cloned.1.call-start = ((), (), s32[]{:S(2)}) async-start(), calls=%async_computation.7 | async-start | bytes 3440640 | tf_op jit(solution)/shard_map/all_gather | solution.py:60
  43.6 20.8 %copy-start.3 = (f32[4,512,128]{2,1,0:T(8,128)S(1)}, f32[4,512,128]{2,1,0:T(8,128)}, u32[]{:S(2)}) copy-start(f32[4,512,128]{2,1,0:T(8,128)} %param.13) | copy-start | bytes 3145732
  60.9 17.0 %all-to-all-start.1 = ((bf16[4,512,128]{2,1,0:T(8,128)(2,1)}), bf16[4,512,128]{2,1,0:T(8,128)(2,1)S(1)}, u32[]{:S(2)}, u32[]{:S(2)}) async-start(bf16[4,512,128]{2,1,0:T(8,128)(2,1)} %get-tuple-element.8), calls=%async_computation.1 | async-start | bytes 1048576 | tf_op jit(solution)/shard_map/all_to_all | solution.py:33
  77.9 4.2 %copy-start.1 = (bf16[4,512,128]{2,1,0:T(8,128)(2,1)}, bf16[4,512,128]{2,1,0:T(8,128)(2,1)S(1)}, u32[]{:S(2)}) copy-start(bf16[4,512,128]{2,1,0:T(8,128)(2,1)S(1)} %all-to-all-done.1) | copy-start | bytes 1572868
  77.9 18.3 %all-to-all-start.2 = ((bf16[4,512,128]{2,1,0:T(8,128)(2,1)}), bf16[4,512,128]{2,1,0:T(8,128)(2,1)}, u32[]{:S(2)}, u32[]{:S(2)}) async-start(bf16[4,512,128]{2,1,0:T(8,128)(2,1)} %convert_element_type.49), calls=%async_computation.2 | async-start | bytes 1048576 | tf_op jit(solution)/shard_map/all_to_all | solution.py:34
  82.0 54.5 %reduce-scatter.2.cloned.1.call-start = ((), (), s32[]{:S(2)}) async-start(), calls=%async_computation.6 | async-start | bytes 3440640 | tf_op jit(solution)/shard_map/reduce_scatter | solution.py:69
  82.1 14.0 %copy-start = (bf16[4,168,2048]{2,1,0:T(8,128)(2,1)S(1)}, bf16[4,168,2048]{2,1,0:T(8,128)(2,1)}, u32[]{:S(2)}) copy-start(bf16[4,168,2048]{2,1,0:T(8,128)(2,1)} %all-gather.3.cloned.1.call-done) | copy-start | bytes 8257540
  102.0 39.1 %copy-start.6 = (f32[224,2]{0,1:T(2,128)S(1)}, f32[224,2]{0,1:T(2,128)}, u32[]{:S(2)}) copy-start(f32[224,2]{0,1:T(2,128)} %param.9) | copy-start | bytes 5380
  102.0 59.2 %copy-start.2 = (bf16[4,512,128]{2,1,0:T(8,128)(2,1)S(1)}, bf16[4,512,128]{2,1,0:T(8,128)(2,1)}, u32[]{:S(2)}) copy-start(bf16[4,512,128]{2,1,0:T(8,128)(2,1)} %copy-done.1) | copy-start | bytes 1572868
  136.5 22.4 %all-to-all-start.4 = ((bf16[512,4,168]{0,2,1:T(8,128)(2,1)}), bf16[512,4,168]{0,2,1:T(8,128)(2,1)S(1)}, u32[]{:S(2)}, u32[]{:S(2)}) async-start(bf16[512,4,168]{0,2,1:T(8,128)(2,1)} %bitcast.47), calls=%async_computation.5 | async-start | bytes 1376256 | tf_op jit(solution)/shard_map/all_to_all | solution.py:77
Sparse Core Ops, SparseCore 0:
  43.7 25.4 all-gather.2
  102.1 34.3 reduce-scatter.1
where the time goes:
time: 171 us
  waiting for transfers between devices  75.5 us (44%)
  blocking collectives  46.2 us (27%)
  between operations  14.2 us (8%)
  starting transfers between devices  12.3 us (7%)
  matrix products  12.3 us (7%)
  other arithmetic  5.18 us (3%)
  local copies, waits for them, and re-layouts  5.04 us (3%)
    reduce_scatter x1, waiting for transfers between devices, local(): lax.psum_scatter(products.reshape(local_width * lax.axis_size('tp'), shar...  34.5 us
    all_to_all x1, blocking collectives, local(): lax.all_to_all(buffer.reshape(shards, per_device * capacity, local_width)...  21.6 us
    all_to_all x1, waiting for transfers between devices, local(): lax.all_to_all(summed.reshape(local_width, shards, per_device * capacity)...  17.8 us
    all_to_all x1, blocking collectives, local(): lax.all_to_all(gate_half, 'fs', split_axis=0, concat_axis=1, tiled=True)  16.2 us
    all_to_all x1, waiting for transfers between devices, local(): lax.all_to_all(up_half, 'fs', split_axis=0, concat_axis=1, tiled=True)  12.6 us
    all_to_all x1, waiting for transfers between devices, local(): lax.all_to_all(down_half, 'fs', split_axis=0, concat_axis=1, tiled=True)  10.5 us
    psum x1, blocking collectives, local(): squares = lax.psum(jnp.sum(local_values * local_values, axis=1), 'tp')  8.37 us
    dot_general x1, matrix products, local(): jnp.einsum('xdf,xscf->dsxc', down_serve, hidden, preferred_element_type=j...  5.82 us
  transfers between devices with their start and end apart: 5, of which 4 were waited for; matrix products, arithmetic and copies ran while one was open for 3% of the time, Pallas kernels for 0%

commit v1 on v0

--- a/solution.py
+++ b/solution.py
@@ -4,6 +4,19 @@
 from jax.sharding import PartitionSpec as P
 
 norm_epsilon = 1e-06
+
+
+def _pack_domain(xs, dim_at, array_in):
+    kept_arr, far_arr = (xs.shape[:dim_at], xs.shape[dim_at + 1 :])
+    row_out = jnp.moveaxis(xs.reshape(*kept_arr, array_in, -1, *far_arr), dim_at, 0)
+    return row_out
+
+
+def pack_side(s0, dimension_no):
+    z2 = list(s0.shape[1:])
+    z2[dimension_no] *= s0.shape[0]
+    block_next = jnp.moveaxis(s0, 0, dimension_no).reshape(z2)
+    return block_next
 
 
 def slot_numbers(route_ids, experts, capacity):
@@ -15,6 +28,21 @@
 
 
 def local(tokens, route_ids, route_weights, norm_gain, gate_master, up_master, down_master):
+
+    def works_fix(xin, which_axis, z_in, block_in=0):
+        top, outcome_arr = (lax.axis_size(which_axis), lax.axis_index(which_axis))
+        latest = _pack_domain(xin, z_in, top)
+        moved = latest
+        for hop_no in range(1, top):
+            field_out, local_out = ((outcome_arr + hop_no) % top, (outcome_arr - hop_no) % top)
+            e_now = lax.dynamic_index_in_dim(latest, field_out, 0)
+            g_now = lax.ppermute(
+                e_now, which_axis, list(map(lambda to_i: (to_i, (to_i + hop_no) % top), range(top)))
+            )
+            moved = lax.dynamic_update_slice_in_dim(moved, g_now, local_out, axis=0)
+        front = pack_side(moved, block_in)
+        return front
+
     experts = gate_master.shape[0]
     shards = lax.axis_size("fs")
     columns = lax.axis_size("tp")
@@ -49,13 +77,7 @@
     buffer = jnp.einsum("ts,td->sd", placing, normed, preferred_element_type=jnp.float32).astype(
         jnp.bfloat16
     )
-    arrived = lax.all_to_all(
-        buffer.reshape(shards, per_device * capacity, local_width),
-        "fs",
-        split_axis=0,
-        concat_axis=0,
-        tiled=True,
-    )
+    arrived = works_fix(buffer.reshape(shards, per_device * capacity, local_width), "fs", 0)
     arrived = arrived.reshape(shards, per_device, capacity, local_width)
     partial_value = lax.all_gather(arrived, "tp", axis=3, tiled=True)
     gate_sum = jnp.einsum(

time: 171 us -> 174 us (1.018)
  blocking collectives: 46.2 us -> 28.4 us
  waiting for transfers between devices: 75.5 us -> 89.7 us
  starting transfers between devices: 12.3 us -> 16.1 us
    all_to_all x2 -> x1, blocking collectives: 37.8 us -> 20 us  [local(): lax.all_to_all(up_half, 'fs', split_axis=0, concat_axis=1, tiled=True)]
    ppermute x0 -> x3, waiting for transfers between devices: none -> 12.9 us  [works_fix(): lax.ppermute(e_now, which_axis, list(map(lambda to_i: (to_i, (to_i + hop_...]
    ppermute x0 -> x3, starting transfers between devices: none -> 3.85 us  [works_fix(): lax.ppermute(e_now, which_axis, list(map(lambda to_i: (to_i, (to_i + hop_...]
  transfers between devices with their start and end apart: 5 -> 8, of which waited for: 4 -> 6; matrix products, arithmetic and copies ran while one was open for 3% -> 4% of each run, Pallas kernels for 0% -> 0%
where the time goes in v1:
time: 174 us; the launch traced here: 173 us
  waiting for transfers between devices  89.7 us (52%)
  blocking collectives  28.4 us (16%)
  starting transfers between devices  16.1 us (9%)
  between operations  14.3 us (8%)
  matrix products  12.3 us (7%)
  other arithmetic  6.49 us (4%)
  local copies, waits for them, and re-layouts  5.92 us (3%)
    reduce_scatter x1, waiting for transfers between devices, local(): lax.psum_scatter(products.reshape(local_width * lax.axis_size('tp'), shar...  35.3 us
    all_to_all x1, blocking collectives, local(): lax.all_to_all(up_half, 'fs', split_axis=0, concat_axis=1, tiled=True)  20 us
    all_to_all x1, waiting for transfers between devices, local(): lax.all_to_all(summed.reshape(local_width, shards, per_device * capacity)...  17.8 us
    all_to_all x1, waiting for transfers between devices, local(): lax.all_to_all(gate_half, 'fs', split_axis=0, concat_axis=1, tiled=True)  13.1 us
    ppermute x3, waiting for transfers between devices, works_fix(): lax.ppermute(e_now, which_axis, list(map(lambda to_i: (to_i, (to_i + hop_...  12.9 us
    all_to_all x1, waiting for transfers between devices, local(): lax.all_to_all(down_half, 'fs', split_axis=0, concat_axis=1, tiled=True)  10.5 us
    psum x1, blocking collectives, local(): squares = lax.psum(jnp.sum(local_values * local_values, axis=1), 'tp')  8.37 us
    dot_general x1, matrix products, local(): jnp.einsum('xdf,xscf->dsxc', down_serve, hidden, preferred_element_type=j...  5.81 us
  transfers between devices with their start and end apart: 8, of which 6 were waited for; matrix products, arithmetic and copies ran while one was open for 4% of the time, Pallas kernels for 0%

profile of v1, /device:TPU:0, one launch (start us, length us, event | category | flops | bytes accessed | tf_op | source)
XLA Modules:
  0.0 173.2 jit_solution(6029193446460293392)
XLA Ops:
  7.2 0.0 copy-start.7
  7.2 0.0 copy-start.5
  7.2 0.0 all-gather.2.cloned.1.call-start
  7.2 0.9 copy.17
  8.1 0.1 eq.59
  8.3 1.2 reduce-window.6
  9.5 0.2 slice_reduce_fusion
  9.8 0.2 reduce-window.9
  9.9 0.1 add_bitcast_fusion
  10.1 0.1 reduce_sum.21
  10.2 0.1 copy.18
  10.3 0.7 multiply_add_fusion
  11.0 1.1 fusion.8
  12.0 8.4 %psum.7 = f32[224]{0:T(256)S(1)} all-reduce(f32[224]{0:T(256)S(1)} %fusion.8), channel_id=1, replica_groups=mesh['grp'=2,'fs'=4,'tp'=4] {'tp'}, use_global_device_ids=true, to_apply=%region_4.5 | all-reduce | flops 224 | bytes 1792 | tf_op jit(solution)/shard_map/psum | solution.py:74
  20.4 1.5 convolution_convert_fusion.1
  21.9 1.6 collective-permute-start
  23.6 5.6 %collective-permute-done = bf16[1,1,168,512]{3,2,0,1:T(8,128)(2,1)S(1)} collective-permute-done((bf16[1,1,168,512]{3,2,0,1:T(8,128)(2,1)S(1)}, bf16[1,1,168,512]{3,2,0,1:T(8,128)(2,1)S(1)}, u32[]{:S(2)}, u32[]{:S(2)}) %collective-permute-start) | collective-permute-done | bytes 172064 | tf_op jit(solution)/shard_map/ppermute | solution.py:39
  29.2 0.1 constant_dynamic-slice_fusion
  29.2 0.9 collective-permute-start.1
  30.1 1.3 collective-permute-start.2
  31.5 7.3 %collective-permute-done.1 = bf16[1,1,168,512]{3,2,0,1:T(8,128)(2,1)S(1)} collective-permute-done((bf16[1,1,168,512]{3,2,0,1:T(8,128)(2,1)S(1)}, bf16[1,1,168,512]{3,2,0,1:T(8,128)(2,1)S(1)}, u32[]{:S(2)}, u32[]{:S(2)}) %collective-permute-start.1) | collective-permute-done | bytes 172064 | tf_op jit(solution)/shard_map/ppermute | solution.py:39
  38.8 0.0 collective-permute-done.2
  38.8 0.0 copy-start.3
  38.8 0.8 copy-done.3
  39.7 0.0 all-gather.2.cloned.1.call-update
  39.7 0.0 copy-done.7
  39.7 0.0 copy-done.5
  39.7 0.0 copy-start.4
  39.7 2.3 %multiply_convert_fusion = (bf16[4,512,128]{2,1,0:T(8,128)(2,1)S(1)}, bf16[4,512,128]{2,1,0:T(8,128)(2,1)}) fusion(f32[4,512,128]{2,1,0:T(8,128)S(1)} %copy-done.5, f32[512]{0:T(512)S(1)} %copy-done.7, f32[4,512,128]{2,1,0:T(8,128)} %param.11), kind=kLoop, calls=%fused_computation.10 | loop fusion | flops 1048576 | bytes 3147776 | tf_op jit(solution)/shard_map/convert_element_type | solution.py:57
  42.1 20.0 %all_to_all.41 = bf16[4,512,128]{2,1,0:T(8,128)(2,1)S(1)} all-to-all(bf16[4,512,128]{2,1,0:T(8,128)(2,1)S(1)} %get-tuple-element.11), channel_id=1, replica_groups=mesh['grp'=2,'fs'=4,'tp'=4] {'fs'}, dimensions={0} | all-to-all | bytes 1048576 | tf_op jit(solution)/shard_map/all_to_all | solution.py:61
  62.1 3.5 %all-to-all-start = ((bf16[4,512,128]{2,1,0:T(8,128)(2,1)}), bf16[4,512,128]{2,1,0:T(8,128)(2,1)S(1)}, u32[]{:S(2)}, u32[]{:S(2)}) async-start(bf16[4,512,128]{2,1,0:T(8,128)(2,1)} %get-tuple-element.12), calls=%async_computation | async-start | bytes 1048576 | tf_op jit(solution)/shard_map/all_to_all | solution.py:60
  65.6 0.0 copy-done.4
  65.6 0.9 convert_element_type.49
  66.4 13.1 %all-to-all-done = bf16[4,512,128]{2,1,0:T(8,128)(2,1)S(1)} async-done(((bf16[4,512,128]{2,1,0:T(8,128)(2,1)}), bf16[4,512,128]{2,1,0:T(8,128)(2,1)S(1)}, u32[]{:S(2)}, u32[]{:S(2)}) %all-to-all-start) | async-done | bytes 524320 | tf_op jit(solution)/shard_map/all_to_all | solution.py:60
  79.6 0.0 copy-start.1
  79.6 4.1 %all-to-all-start.2 = ((bf16[4,512,128]{2,1,0:T(8,128)(2,1)}), bf16[4,512,128]{2,1,0:T(8,128)(2,1)}, u32[]{:S(2)}, u32[]{:S(2)}) async-start(bf16[4,512,128]{2,1,0:T(8,128)(2,1)} %convert_element_type.49), calls=%async_computation.2 | async-start | bytes 1048576 | tf_op jit(solution)/shard_map/all_to_all | solution.py:62
  83.7 0.0 reduce-scatter.2.cloned.1.call-start
  83.8 0.0 copy-done.1
  83.8 0.0 all-gather.2.cloned.1.call-done
  83.8 0.0 copy-start
  83.8 3.5 %fusion = f32[4,168,128]{2,1,0:T(8,128)} fusion(bf16[2048,128,1]{1,0,2:T(8,128)(2,1)S(1)} %bitcast.48, bf16[4,1,168,2048]{3,2,0,1:T(8,128)(2,1)} %all-gather.2.cloned.1.call-done), kind=kOutput, calls=%fused_computation.1 | convolution fusion | flops 352321536 | bytes 3620864 | tf_op jit(solution)/shard_map/sxcd,xdf->xscf/dot_general | solution.py:86
  87.4 10.5 %all-to-all-done.2 = bf16[4,512,128]{2,1,0:T(8,128)(2,1)} async-done(((bf16[4,512,128]{2,1,0:T(8,128)(2,1)}), bf16[4,512,128]{2,1,0:T(8,128)(2,1)}, u32[]{:S(2)}, u32[]{:S(2)}) %all-to-all-start.2) | async-done | bytes 524320 | tf_op jit(solution)/shard_map/all_to_all | solution.py:62
  97.8 0.0 copy-done
  97.8 5.8 %convolution_convert_fusion = bf16[4,168,2048]{2,1,0:T(8,128)(2,1)} fusion(bf16[2048,128,1]{1,0,2:T(8,128)(2,1)} %bitcast.14, f32[4,168,128]{2,1,0:T(8,128)} %fusion, bf16[2048,128,1]{1,0,2:T(8,128)(2,1)} %bitcast.50, bf16[4,1,168,2048]{3,2,0,1:T(8,128)(2,1)S(1)} %copy-done), kind=kOutput, calls=%fused_computation | convolution fusion | flops 706535424 | bytes 6897664 | tf_op jit(solution)/shard_map/xdf,xscf->dsxc/dot_general | solution.py:90
  103.7 0.0 copy-start.6
  103.7 0.0 copy-start.2
  103.7 0.0 reduce-scatter.2.cloned.1.call-update
  103.7 35.3 %reduce-scatter.2.cloned.1.call-done = bf16[512,672]{0,1:T(8,128)(2,1)} async-done(((bf16[2048,672]{0,1:T(8,128)(2,1)}), bf16[512,672]{0,1:T(8,128)(2,1)}) %reduce-scatter.2.cloned.1.call-update) | async-done | bytes 688144 | tf_op jit(solution)/shard_map/reduce_scatter | solution.py:91
  138.9 4.6 %all-to-all-start.3 = ((bf16[512,4,168]{0,2,1:T(8,128)(2,1)}), bf16[512,4,168]{0,2,1:T(8,128)(2,1)S(1)}, u32[]{:S(2)}, u32[]{:S(2)}) async-start(bf16[512,4,168]{0,2,1:T(8,128)(2,1)} %bitcast.56), calls=%async_computation.4 | async-start | bytes 1376256 | tf_op jit(solution)/shard_map/all_to_all | solution.py:99
  143.6 0.0 copy-done.6
  143.6 17.8 %all-to-all-done.3 = bf16[512,4,168]{0,2,1:T(8,128)(2,1)S(1)} async-done(((bf16[512,4,168]{0,2,1:T(8,128)(2,1)}), bf16[512,4,168]{0,2,1:T(8,128)(2,1)S(1)}, u32[]{:S(2)}, u32[]{:S(2)}) %all-to-all-start.3) | async-done | bytes 688160 | tf_op jit(solution)/shard_map/all_to_all | solution.py:99
  161.4 0.4 convolution_multiply_fusion.1
  161.8 1.1 fusion.5
  162.9 0.0 copy-done.2
  162.9 0.8 copy.28
  163.7 0.8 copy.29
  164.5 1.9 %copy.30 = bf16[1,2048,128]{2,1,0:T(8,128)(2,1)} copy(bf16[1,2048,128]{2,1,0:T(8,128)(2,1)} %bitcast.2) | data formatting | bytes 1048576
  (11 shorter events, 0.1 us)
Async XLA Ops:
  7.2 32.5 %copy-start.7 = (f32[512]{0:T(512)S(1)}, f32[512]{0:T(512)}, u32[]{:S(2)}) copy-start(f32[512]{0:T(512)} %param.10) | copy-start | bytes 6148
  7.2 32.5 %copy-start.5 = (f32[4,512,128]{2,1,0:T(8,128)S(1)}, f32[4,512,128]{2,1,0:T(8,128)}, u32[]{:S(2)}) copy-start(f32[4,512,128]{2,1,0:T(8,128)} %param.12) | copy-start | bytes 3145732
  7.2 76.6 %all-gather.2.cloned.1.call-start = ((), (), s32[]{:S(2)}) async-start(), calls=%async_computation.5 | async-start | bytes 3440640 | tf_op jit(solution)/shard_map/all_gather | solution.py:82
  21.9 7.3 %collective-permute-start = (bf16[1,1,168,512]{3,2,0,1:T(8,128)(2,1)S(1)}, bf16[1,1,168,512]{3,2,0,1:T(8,128)(2,1)S(1)}, u32[]{:S(2)}, u32[]{:S(2)}) collective-permute-start(bf16[1,1,168,512]{3,2,0,1:T(8,128)(2,1)S(1)} %constant_dynamic-slice_fusion.2), channel_id=1, source_target_pairs={{0,4},{4,8},{8,12},{12,0},{1,5},{5,9},{9,13},{13,1},{2,6},{6,10},{... | collective-permute-start | bytes 516104 | tf_op jit(solution)/shard_map/ppermute | solution.py:39
  29.2 9.5 %collective-permute-start.1 = (bf16[1,1,168,512]{3,2,0,1:T(8,128)(2,1)S(1)}, bf16[1,1,168,512]{3,2,0,1:T(8,128)(2,1)S(1)}, u32[]{:S(2)}, u32[]{:S(2)}) collective-permute-start(bf16[1,1,168,512]{3,2,0,1:T(8,128)(2,1)S(1)} %get-tuple-element.5), channel_id=1, source_target_pairs={{0,8},{4,12},{8,0},{12,4},{1,9},{5,13},{9,1},{13,5},{2,10},{6,14},... | collective-permute-start | bytes 516104 | tf_op jit(solution)/shard_map/ppermute | solution.py:39
  30.1 8.7 %collective-permute-start.2 = (bf16[1,1,168,512]{3,2,0,1:T(8,128)(2,1)S(1)}, bf16[1,1,168,512]{3,2,0,1:T(8,128)(2,1)S(1)}, u32[]{:S(2)}, u32[]{:S(2)}) collective-permute-start(bf16[1,1,168,512]{3,2,0,1:T(8,128)(2,1)S(1)} %get-tuple-element.4), channel_id=1, source_target_pairs={{0,12},{4,0},{8,4},{12,8},{1,13},{5,1},{9,5},{13,9},{2,14},{6,2},{... | collective-permute-start | bytes 516104 | tf_op jit(solution)/shard_map/ppermute | solution.py:39
  38.8 0.8 copy-start.3
  39.7 25.8 %copy-start.4 = (f32[4,512,128]{2,1,0:T(8,128)S(1)}, f32[4,512,128]{2,1,0:T(8,128)}, u32[]{:S(2)}) copy-start(f32[4,512,128]{2,1,0:T(8,128)} %param.13) | copy-start | bytes 3145732
  62.1 17.5 %all-to-all-start = ((bf16[4,512,128]{2,1,0:T(8,128)(2,1)}), bf16[4,512,128]{2,1,0:T(8,128)(2,1)S(1)}, u32[]{:S(2)}, u32[]{:S(2)}) async-start(bf16[4,512,128]{2,1,0:T(8,128)(2,1)} %get-tuple-element.12), calls=%async_computation | async-start | bytes 1048576 | tf_op jit(solution)/shard_map/all_to_all | solution.py:60
  79.6 4.2 %copy-start.1 = (bf16[4,512,128]{2,1,0:T(8,128)(2,1)}, bf16[4,512,128]{2,1,0:T(8,128)(2,1)S(1)}, u32[]{:S(2)}) copy-start(bf16[4,512,128]{2,1,0:T(8,128)(2,1)S(1)} %all-to-all-done) | copy-start | bytes 1572868
  79.6 18.3 %all-to-all-start.2 = ((bf16[4,512,128]{2,1,0:T(8,128)(2,1)}), bf16[4,512,128]{2,1,0:T(8,128)(2,1)}, u32[]{:S(2)}, u32[]{:S(2)}) async-start(bf16[4,512,128]{2,1,0:T(8,128)(2,1)} %convert_element_type.49), calls=%async_computation.2 | async-start | bytes 1048576 | tf_op jit(solution)/shard_map/all_to_all | solution.py:62
  83.7 55.2 %reduce-scatter.2.cloned.1.call-start = ((), (), s32[]{:S(2)}) async-start(), calls=%async_computation.6 | async-start | bytes 3440640 | tf_op jit(solution)/shard_map/reduce_scatter | solution.py:91
  83.8 14.0 %copy-start = (bf16[4,1,168,2048]{3,2,0,1:T(8,128)(2,1)S(1)}, bf16[4,1,168,2048]{3,2,0,1:T(8,128)(2,1)}, u32[]{:S(2)}) copy-start(bf16[4,1,168,2048]{3,2,0,1:T(8,128)(2,1)} %all-gather.2.cloned.1.call-done) | copy-start | bytes 8257540
  103.7 39.9 %copy-start.6 = (f32[224,2]{0,1:T(2,128)S(1)}, f32[224,2]{0,1:T(2,128)}, u32[]{:S(2)}) copy-start(f32[224,2]{0,1:T(2,128)} %param.9) | copy-start | bytes 5380
  103.7 59.2 %copy-start.2 = (bf16[4,512,128]{2,1,0:T(8,128)(2,1)S(1)}, bf16[4,512,128]{2,1,0:T(8,128)(2,1)}, u32[]{:S(2)}) copy-start(bf16[4,512,128]{2,1,0:T(8,128)(2,1)} %copy-done.1) | copy-start | bytes 1572868
  138.9 22.4 %all-to-all-start.3 = ((bf16[512,4,168]{0,2,1:T(8,128)(2,1)}), bf16[512,4,168]{0,2,1:T(8,128)(2,1)S(1)}, u32[]{:S(2)}, u32[]{:S(2)}) async-start(bf16[512,4,168]{0,2,1:T(8,128)(2,1)} %bitcast.56), calls=%async_computation.4 | async-start | bytes 1376256 | tf_op jit(solution)/shard_map/all_to_all | solution.py:99
Sparse Core Ops, SparseCore 0:
  39.8 29.0 all-gather.1
  103.8 35.1 reduce-scatter.1
